TPU v7x, 512 devices: a whole 4x4x16 slice. The times are simulated.
512 devices in a mesh: ep: 128 (over z, x, core), tp: 4 (over y).
Axes of the slice: x: 4, y: 4, z: 16, core: 2. Of those that a mesh axis runs over, the one named last changes fastest.
Arguments:
- tokens: bfloat16 [1024, 2048], P('ep'), may hold values from -6 to 6
- norm_gain: float32 [2048], replicated, may hold values from 0.1 to 1.9
- query_weight: bfloat16 [2048, 1024], P('ep', 'tp'), may hold values from -0.125 to 0.125
- key_weight: bfloat16 [2048, 512], P('ep', 'tp'), may hold values from -0.125 to 0.125
- value_weight: bfloat16 [2048, 512], P('ep', 'tp'), may hold values from -0.125 to 0.125
- query_gain: float32 [64], replicated, may hold values from 0.9 to 1.9
- key_gain: float32 [64], replicated, may hold values from 0.9 to 1.9
- lambdas: float32 [8], P('tp'), may hold values from 0.3 to 0.8
- key_cache: bfloat16 [1024, 4, 320, 128], P('ep', 'tp'), may hold values from -5 to 5
- value_cache: bfloat16 [1024, 4, 320, 128], P('ep', 'tp'), may hold values from -6 to 6
- lengths: int32 [1024], P('ep'), may hold values from 1 to 320
- head_gain: float32 [128], replicated, may hold values from 0.1 to 1.9
- out_weight: bfloat16 [1024, 2048], P('tp', 'ep'), may hold values from -0.1875 to 0.1875
- ffn_gain: float32 [2048], replicated, may hold values from 0.1 to 1.9
- dense_gate_weight: bfloat16 [2048, 1024], P('ep', 'tp'), may hold values from -0.125 to 0.125
- dense_up_weight: bfloat16 [2048, 1024], P('ep', 'tp'), may hold values from -0.125 to 0.125
- dense_down_weight: bfloat16 [1024, 2048], P('tp', 'ep'), may hold values from -0.1875 to 0.1875
- branch_gate: float32 [2048], replicated, may hold values from -0.125 to 0.125
- expert_ids: int32 [1024, 2], P('ep'), may hold values from 0 to 15, all different within a row; in each aligned block of 8 rows (0 to 7, 8 to 15, ...) at most 2 rows name the same one
- expert_probs: float32 [1024, 2], P('ep'), may hold values from 0.1 to 0.9
- expert_gate: bfloat16 [128, 2048, 704], P('ep', None, 'tp'), may hold values from -0.125 to 0.125
- expert_up: bfloat16 [128, 2048, 704], P('ep', None, 'tp'), may hold values from -0.125 to 0.125
- expert_down: bfloat16 [128, 704, 2048], P('ep', 'tp'), may hold values from -0.078125 to 0.078125
Outputs:
- mixed: bfloat16 [1024, 2048], P('ep', 'tp')
Inputs may be any that keep to these rules, and one draw needn't show every extreme that they name: `expert_ids`: each row names 2 different experts. Within each aligned block of 8 rows (the sequences of one index of ep) no expert is named more than 2 times, and in every draw some block names some expert exactly 2 times.
All inputs are finite; a program needn't handle non-finite values.
Results may differ from a plain program's by a relative error of at most 0.014.
Values may be sent and summed in bfloat16 or wider, within the bound.
No kernel may reach another device: no remote copies, remote signals or barrier semaphores. Data moves between devices by JAX's collectives and lax.ppermute only.
A program may use at most 64 MiB of HBM per device.

v0:
```python
import jax
import jax.numpy as jnp
from jax import lax
from jax.sharding import Mesh, PartitionSpec as P

SUB = 64
VD = 128
EXPERTS = 16
TOP = 2
CAP = 2
REP = 8
N_Z = 16
N_XC = 8
N_EP = 128
N_TP = 4
SEQ = 8
EP = ("b", "zp", "x", "c")
Z = ("b", "zp")
XC = ("x", "c")
epsilon = 1e-06


def rms_scale(values, scaling):
    return values * lax.rsqrt(jnp.mean(values * values, axis=-1, keepdims=True) + epsilon) * scaling


def exchange(values, axes):
    return lax.all_to_all(values, axes, split_axis=0, concat_axis=0, tiled=True)


def gather_small(values, axes, count):
    return exchange(jnp.broadcast_to(values[None], (count,) + values.shape), axes)


def to_mixed(rows):
    count = rows.shape[0]
    return rows.reshape(count, N_Z, N_XC, -1).transpose(0, 2, 1, 3).reshape(count, -1)


def from_mixed(rows):
    count = rows.shape[0]
    return rows.reshape(count, N_XC, N_Z, -1).transpose(0, 2, 1, 3).reshape(count, -1)


def attend(packed, key_cache, value_cache, lengths, query_gain, key_gain, lambdas, head_gain):
    seq_here = packed.shape[0]
    kv_here = key_cache.shape[1]
    cache_len = key_cache.shape[2]
    heads_here = lambdas.shape[0]
    per_group = heads_here // kv_here
    query_end = heads_here * 2 * SUB
    key_end = query_end + kv_here * 2 * SUB
    mixed = lax.optimization_barrier(packed.astype(jnp.bfloat16))
    query_parts = rms_scale(
        mixed[:, :query_end].astype(jnp.float32).reshape(seq_here, kv_here, per_group, 2, SUB),
        query_gain,
    ).astype(jnp.bfloat16)
    key_parts = rms_scale(
        mixed[:, query_end:key_end].astype(jnp.float32).reshape(seq_here, kv_here, 2, SUB), key_gain
    ).astype(jnp.bfloat16)
    new_values = mixed[:, key_end:].reshape(seq_here, kv_here, VD)
    cached = rms_scale(
        key_cache.astype(jnp.float32).reshape(seq_here, kv_here, cache_len, 2, SUB), key_gain
    ).astype(jnp.bfloat16)
    score_scale = SUB ** (-0.5)
    scores = (
        jnp.einsum("sgqcd,sgjcd->sgqcj", query_parts, cached, preferred_element_type=jnp.float32)
        * score_scale
    )
    own_score = (
        jnp.einsum("sgqcd,sgcd->sgqc", query_parts, key_parts, preferred_element_type=jnp.float32)
        * score_scale
    )
    live_mask = lax.broadcasted_iota(jnp.int32, (seq_here, cache_len), 1) < lengths[:, None]
    exponent = jnp.where(live_mask[:, None, None, None, :], jnp.exp(scores), 0.0)
    own_exponent = jnp.exp(own_score)
    denominator = jnp.sum(exponent, axis=4) + own_exponent
    shares = exponent / denominator[..., None]
    own_shares = own_exponent / denominator
    lam_heads = lambdas.reshape(1, kv_here, per_group)
    mixing = (shares[:, :, :, 0] - lam_heads[..., None] * shares[:, :, :, 1]).astype(jnp.bfloat16)
    own_mixing = lax.optimization_barrier(
        (own_shares[:, :, :, 0] - lam_heads * own_shares[:, :, :, 1]).astype(jnp.bfloat16)
    )
    head_out = jnp.einsum(
        "sgqj,sgje->sgqe", mixing, value_cache, preferred_element_type=jnp.float32
    )
    head_out = (
        head_out
        + own_mixing.astype(jnp.float32)[..., None] * new_values.astype(jnp.float32)[:, :, None, :]
    )
    return rms_scale(head_out, head_gain).astype(jnp.bfloat16).reshape(seq_here, heads_here * VD)


def route_tables(expert_ids, expert_probs):
    seq_here = expert_ids.shape[0]
    paired = expert_ids.reshape(-1)
    total_pairs = paired.shape[0]
    onehot = (paired[:, None] == lax.broadcasted_iota(jnp.int32, (total_pairs, EXPERTS), 1)).astype(
        jnp.float32
    )
    earlier = (
        lax.broadcasted_iota(jnp.int32, (total_pairs, total_pairs), 1)
        < lax.broadcasted_iota(jnp.int32, (total_pairs, total_pairs), 0)
    ).astype(jnp.float32)
    before = jnp.dot(earlier, onehot, precision=lax.Precision.HIGHEST)
    slot_ranks = jnp.sum(before * onehot, axis=1).astype(jnp.int32)
    slot_codes = (paired * CAP + slot_ranks).reshape(seq_here, TOP)
    slots_iota = lax.broadcasted_iota(jnp.int32, (seq_here, TOP, EXPERTS * CAP), 2)
    picked = (slot_codes[:, :, None] == slots_iota).astype(jnp.float32)
    select = jnp.sum(picked, axis=1)
    combine_weights = jnp.sum(picked * expert_probs[:, :, None], axis=1)
    return (select, combine_weights)


def own_columns(values, tp_start, share_width):
    return lax.dynamic_slice_in_dim(values, tp_start, share_width, 1)


def shards(
    tokens,
    norm_gain,
    query_weight,
    key_weight,
    value_weight,
    query_gain,
    key_gain,
    lambdas,
    key_cache,
    value_cache,
    lengths,
    head_gain,
    out_weight,
    ffn_gain,
    dense_gate_weight,
    dense_up_weight,
    dense_down_weight,
    branch_gate,
    expert_ids,
    expert_probs,
    expert_gate,
    expert_up,
    expert_down,
):
    residual = tokens.astype(jnp.float32)
    normed = rms_scale(residual, norm_gain).astype(jnp.bfloat16)
    width = residual.shape[1]
    share_width = width // N_TP
    tp_start = lax.axis_index("tp") * share_width
    spread = exchange(
        to_mixed(normed).reshape(SEQ, N_XC, width // N_XC).transpose(1, 0, 2), XC
    ).reshape(N_XC * SEQ, width // N_XC)
    shard = jnp.concatenate(
        (
            query_weight,
            key_weight,
            value_weight,
            out_weight.T,
            dense_gate_weight,
            dense_up_weight,
            dense_down_weight.T,
        ),
        axis=1,
    )
    held = lax.all_gather(shard, Z, axis=0, tiled=True)
    out_held = lax.all_gather(held[:, 512:768], XC, axis=0, tiled=True)
    dense_held = lax.all_gather(held[:, 768:], XC, axis=0, tiled=True)
    partial_rows = jnp.dot(spread, held[:, :512], preferred_element_type=jnp.float32)
    packed = jnp.sum(exchange(partial_rows.reshape(N_XC, SEQ, 512), XC), axis=0)
    head_out = attend(
        packed, key_cache, value_cache, lengths, query_gain, key_gain, lambdas, head_gain
    )
    attended_part = from_mixed(
        lax.dot_general(
            head_out, out_held, (((1,), (1,)), ((), ())), preferred_element_type=jnp.float32
        ).astype(jnp.bfloat16)
    )
    attended = jnp.sum(gather_small(attended_part, "tp", N_TP).astype(jnp.float32), axis=0)
    middle = lax.optimization_barrier((residual + attended).astype(jnp.bfloat16))
    middle_f32 = middle.astype(jnp.float32)
    ffn_input = lax.optimization_barrier(rms_scale(middle_f32, ffn_gain).astype(jnp.bfloat16))
    select, combine_weights = route_tables(expert_ids, expert_probs)
    ffn_share = own_columns(ffn_input, tp_start, share_width)
    chosen = jnp.dot(
        select.astype(jnp.bfloat16).T, ffn_share, preferred_element_type=jnp.float32
    ).astype(jnp.bfloat16)
    outgoing = jnp.broadcast_to(
        chosen.reshape(1, EXPERTS, CAP, share_width), (REP, EXPERTS, CAP, share_width)
    ).reshape(N_EP, CAP, share_width)
    incoming = exchange(outgoing, EP).reshape(N_EP * CAP, share_width)
    dense_both = jnp.dot(
        to_mixed(ffn_input), dense_held[:, :512], preferred_element_type=jnp.float32
    )
    dense_hidden = (jax.nn.silu(dense_both[:, :256]) * dense_both[:, 256:]).astype(jnp.bfloat16)
    dense_part = from_mixed(
        lax.dot_general(
            dense_hidden,
            dense_held[:, 512:],
            (((1,), (1,)), ((), ())),
            preferred_element_type=jnp.float32,
        ).astype(jnp.bfloat16)
    )
    branch_weight = jax.nn.sigmoid(
        jnp.sum(ffn_input.astype(jnp.float32) * branch_gate, axis=1, keepdims=True)
    )
    rows = gather_small(incoming, "tp", N_TP)
    rows = rows.transpose(1, 0, 2).reshape(N_EP * CAP, width)
    gate_val = jnp.dot(rows, expert_gate[0], preferred_element_type=jnp.float32)
    up_val = jnp.dot(rows, expert_up[0], preferred_element_type=jnp.float32)
    hidden = (jax.nn.silu(gate_val) * up_val).astype(jnp.bfloat16)
    expert_part = jnp.dot(hidden, expert_down[0], preferred_element_type=jnp.float32).astype(
        jnp.bfloat16
    )
    both_parts = jnp.concatenate((expert_part, dense_part), axis=0)
    both_parts = both_parts.reshape(N_EP * CAP + SEQ, N_TP, share_width).transpose(1, 0, 2)
    summed = jnp.sum(exchange(both_parts, "tp").astype(jnp.float32), axis=0)
    block_out = summed[: N_EP * CAP].astype(jnp.bfloat16).reshape(N_EP, CAP, share_width)
    dense = summed[N_EP * CAP :]
    returned = exchange(block_out, EP)
    expert_out = jnp.sum(
        returned.reshape(REP, EXPERTS * CAP, share_width).astype(jnp.float32), axis=0
    )
    routed = jnp.dot(combine_weights, expert_out, precision=lax.Precision.HIGHEST)
    combined = own_columns(middle_f32, tp_start, share_width) + branch_weight * dense + routed
    return combined.astype(jnp.bfloat16)


def solution(mesh):
    fine = Mesh(mesh.devices.reshape(8, 2, 4, 2, 4), ("b", "zp", "x", "c", "tp"))
    return jax.shard_map(
        shards,
        mesh=fine,
        in_specs=(
            P(EP, None),
            P(),
            P(EP, "tp"),
            P(EP, "tp"),
            P(EP, "tp"),
            P(),
            P(),
            P("tp"),
            P(EP, "tp", None, None),
            P(EP, "tp", None, None),
            P(EP),
            P(),
            P("tp", EP),
            P(),
            P(EP, "tp"),
            P(EP, "tp"),
            P("tp", EP),
            P(),
            P(EP, None),
            P(EP, None),
            P(EP, None, "tp"),
            P(EP, None, "tp"),
            P(EP, "tp", None),
        ),
        out_specs=P(EP, "tp"),
        check_vma=False,
    )
```

profile of v0, /device:TPU:33, one launch (start us, length us, event | category | flops | bytes accessed | tf_op | source)
XLA Modules:
  0.0 216.1 jit_solution(8337824748790621756)
XLA Ops:
  6.5 0.8 constant_dynamic-update-slice_fusion.6
  7.3 0.7 constant_dynamic-update-slice_fusion.5
  8.0 0.7 constant_dynamic-update-slice_fusion.4
  8.7 0.7 constant_dynamic-update-slice_fusion.3
  9.4 0.7 constant_dynamic-update-slice_fusion.2
  10.1 0.7 constant_dynamic-update-slice_fusion.1
  10.8 0.7 constant_dynamic-update-slice_fusion
  11.5 30.8 %all_gather.9 = bf16[256,1536]{1,0:T(8,128)(2,1)S(1)} all-gather(bf16[16,1536]{1,0:T(8,128)(2,1)S(1)} %constant_dynamic-update-slice_fusion), channel_id=1, replica_groups=mesh['b'=8,'zp'=2,'x'=4,'c'=2,'tp'=4] {'b','zp'}, dimensions={0}, use_global_device_ids=true | all-gather | bytes 835584 | tf_op jit(solution)/shard_map/all_gather | solution.py:165
  42.3 0.7 slice.73
  43.0 0.9 fusion.25
  43.9 0.8 fusion.27
  44.7 0.2 reshape.334
  45.0 0.8 reshape_reshape.3
  45.8 11.8 %all-to-all-start = ((bf16[8,8,256]{2,1,0:T(8,128)(2,1)}), bf16[8,8,256]{2,1,0:T(8,128)(2,1)S(1)}, u32[]{:S(2)}, u32[]{:S(2)}) async-start(bf16[8,8,256]{2,1,0:T(8,128)(2,1)} %bitcast.3), calls=%async_computation | async-start | bytes 65536 | tf_op jit(solution)/shard_map/all_to_all | solution.py:28
  57.7 0.8 slice.74
  58.5 1.2 copy.94
  59.6 1.3 convert_multiply_fusion
  61.0 0.2 reduce_sum.137
  61.3 0.1 fusion.6
  61.7 0.7 all-to-all-done
  62.4 0.8 fusion.18
  63.2 4.1 %all-to-all-start.1 = ((f32[8,8,512]{2,1,0:T(8,128)}), f32[8,8,512]{2,1,0:T(8,128)S(1)}, u32[]{:S(2)}, u32[]{:S(2)}) async-start(f32[8,8,512]{2,1,0:T(8,128)} %fusion.18), calls=%async_computation.1 | async-start | bytes 262144 | tf_op jit(solution)/shard_map/all_to_all | solution.py:28
  67.4 6.1 %all-to-all-done.1 = f32[8,8,512]{2,1,0:T(8,128)S(1)} async-done(((f32[8,8,512]{2,1,0:T(8,128)}), f32[8,8,512]{2,1,0:T(8,128)S(1)}, u32[]{:S(2)}, u32[]{:S(2)}) %all-to-all-start.1) | async-done | bytes 131104 | tf_op jit(solution)/shard_map/all_to_all | solution.py:28
  73.8 0.1 reduce_sum.140
  74.2 0.1 fusion.36
  74.4 0.1 copy.112
  74.5 1.6 fusion.57
  76.1 0.1 copy.97
  76.3 0.1 copy.99
  76.4 0.1 broadcast_divide_fusion
  76.6 0.3 multiply_reduce_fusion.2
  77.0 2.3 %all-gather.3.cloned.1.call-done = bf16[2048,256]{1,0:T(8,128)(2,1)} async-done(((bf16[256,256]{1,0:T(8,128)(2,1)}), bf16[2048,256]{1,0:T(8,128)(2,1)}) %all-gather.3.cloned.1.call-update) | async-done | bytes 1048592 | tf_op jit(solution)/shard_map/all_gather | solution.py:166
  79.4 1.6 convolution_convert_fusion.2
  80.9 0.2 reshape.339
  81.3 0.3 broadcast_in_dim.26
  81.6 0.7 broadcast_in_dim.27
  82.2 4.0 %all-to-all-start.2 = ((bf16[4,8,2048]{2,1,0:T(8,128)(2,1)}), bf16[4,8,2048]{2,1,0:T(8,128)(2,1)S(1)}, u32[]{:S(2)}, u32[]{:S(2)}) async-start(bf16[4,8,2048]{2,1,0:T(8,128)(2,1)} %broadcast_in_dim.27), calls=%async_computation.2 | async-start | bytes 262144 | tf_op jit(solution)/shard_map/all_to_all | solution.py:28
  86.3 4.7 %all-to-all-done.2 = bf16[4,8,2048]{2,1,0:T(8,128)(2,1)S(1)} async-done(((bf16[4,8,2048]{2,1,0:T(8,128)(2,1)}), bf16[4,8,2048]{2,1,0:T(8,128)(2,1)S(1)}, u32[]{:S(2)}, u32[]{:S(2)}) %all-to-all-start.2) | async-done | bytes 131104 | tf_op jit(solution)/shard_map/all_to_all | solution.py:28
  91.1 0.1 multiply_reduce_fusion.1
  91.3 0.5 copy-done.3
  91.8 0.2 convolution_convert_fusion.3
  92.0 0.1 broadcast_in_dim.29
  92.2 39.2 %all_to_all.35 = bf16[128,2,512]{2,1,0:T(2,128)(2,1)S(1)} all-to-all(bf16[128,2,512]{2,1,0:T(2,128)(2,1)S(1)} %bitcast.137), channel_id=1, replica_groups=mesh['b'=8,'zp'=2,'x'=4,'c'=2,'tp'=4] {'b','zp','x','c'}, dimensions={0} | all-to-all | bytes 524288 | tf_op jit(solution)/shard_map/all_to_all | solution.py:28
  131.3 0.1 broadcast_in_dim.30
  131.4 0.1 copy.106
  131.6 1.1 broadcast_in_dim.31
  132.6 3.5 %all-to-all-start.4 = ((bf16[4,256,512]{1,2,0:T(8,128)(2,1)}), bf16[4,256,512]{1,2,0:T(8,128)(2,1)S(1)}, u32[]{:S(2)}, u32[]{:S(2)}) async-start(bf16[4,256,512]{1,2,0:T(8,128)(2,1)} %broadcast_in_dim.31), calls=%async_computation.4 | async-start | bytes 2097152 | tf_op jit(solution)/shard_map/all_to_all | solution.py:28
  136.2 0.2 reshape.342
  136.4 0.9 reshape.343
  137.4 13.6 %all-to-all-done.4 = bf16[4,256,512]{1,2,0:T(8,128)(2,1)S(1)} async-done(((bf16[4,256,512]{1,2,0:T(8,128)(2,1)}), bf16[4,256,512]{1,2,0:T(8,128)(2,1)S(1)}, u32[]{:S(2)}, u32[]{:S(2)}) %all-to-all-start.4) | async-done | bytes 1048608 | tf_op jit(solution)/shard_map/all_to_all | solution.py:28
  151.0 2.1 fusion.15
  153.1 2.1 convolution_convert_fusion
  155.4 0.6 copy-done.8
  156.0 2.0 fusion
  157.9 1.6 convolution_convert_fusion.1
  159.5 0.2 reshape.344
  159.9 0.3 concatenate.13
  160.3 16.8 %all_to_all.36 = bf16[4,264,512]{2,1,0:T(8,128)(2,1)S(1)} all-to-all(bf16[4,264,512]{2,1,0:T(8,128)(2,1)S(1)} %maximum_bitcast_fusion), channel_id=1, replica_groups=mesh['b'=8,'zp'=2,'x'=4,'c'=2,'tp'=4] {'tp'}, dimensions={0} | all-to-all | bytes 2162688 | tf_op jit(solution)/shard_map/all_to_all | solution.py:28
  177.0 0.2 convert_reduce_fusion
  177.2 0.8 reshape.345
  178.0 7.7 %all-to-all-start.6 = ((bf16[128,2,512]{2,1,0:T(2,128)(2,1)}), bf16[128,2,512]{2,1,0:T(2,128)(2,1)S(1)}, u32[]{:S(2)}, u32[]{:S(2)}) async-start(bf16[128,2,512]{2,1,0:T(2,128)(2,1)} %reshape.345), calls=%async_computation.6 | async-start | bytes 524288 | tf_op jit(solution)/shard_map/all_to_all | solution.py:28
  185.8 0.1 multiply_reduce_fusion
  185.9 22.4 %all-to-all-done.6 = bf16[128,2,512]{2,1,0:T(2,128)(2,1)S(1)} async-done(((bf16[128,2,512]{2,1,0:T(2,128)(2,1)}), bf16[128,2,512]{2,1,0:T(2,128)(2,1)S(1)}, u32[]{:S(2)}, u32[]{:S(2)}) %all-to-all-start.6) | async-done | bytes 262176 | tf_op jit(solution)/shard_map/all_to_all | solution.py:28
  208.5 0.8 fusion.5
  (90 shorter events, 2.2 us)
Async XLA Ops:
  6.5 146.6 %copy-start = (bf16[1,176,2048]{2,1,0:T(8,128)(2,1)S(1)}, bf16[1,176,2048]{2,1,0:T(8,128)(2,1)}, u32[]{:S(2)}) copy-start(bf16[1,176,2048]{2,1,0:T(8,128)(2,1)} %param.45) | copy-start | bytes 2162692
  6.5 72.8 %all-gather.3.cloned.1.call-start = ((), (), s32[]{:S(2)}) async-start(), calls=%async_computation.7 | async-start | bytes 1179648 | tf_op jit(solution)/shard_map/all_gather | solution.py:166
  42.3 16.2 %copy-start.2 = (bf16[8,1,320,128]{3,2,1,0:T(8,128)(2,1)S(1)}, bf16[8,1,320,128]{3,2,1,0:T(8,128)(2,1)}, u32[]{:S(2)}) copy-start(bf16[8,1,320,128]{3,2,1,0:T(8,128)(2,1)} %param.31) | copy-start | bytes 1966084
  45.8 16.5 %all-to-all-start = ((bf16[8,8,256]{2,1,0:T(8,128)(2,1)}), bf16[8,8,256]{2,1,0:T(8,128)(2,1)S(1)}, u32[]{:S(2)}, u32[]{:S(2)}) async-start(bf16[8,8,256]{2,1,0:T(8,128)(2,1)} %bitcast.3), calls=%async_computation | async-start | bytes 65536 | tf_op jit(solution)/shard_map/all_to_all | solution.py:28
  57.7 97.7 %all-gather.5.cloned.1.call-start = ((), (), s32[]{:S(2)}) async-start(), calls=%async_computation.8 | async-start | bytes 3538944 | tf_op jit(solution)/shard_map/all_gather | solution.py:167
  59.6 1.5 copy-start.11
  60.9 6.4 %copy-start.14 = (s32[8]{0:T(128)S(1)}, s32[8]{0:T(128)}, u32[]{:S(2)}) copy-start(s32[8]{0:T(128)} %param.33) | copy-start | bytes 100
  60.9 13.1 %copy-start.15 = (f32[64]{0:T(128)S(1)}, f32[64]{0:T(128)}, u32[]{:S(2)}) copy-start(f32[64]{0:T(128)} %param.29) | copy-start | bytes 772
  60.9 13.2 %copy-start.13 = (f32[64]{0:T(128)S(1)}, f32[64]{0:T(128)}, u32[]{:S(2)}) copy-start(f32[64]{0:T(128)} %param.28) | copy-start | bytes 772
  61.1 15.1 %copy-start.17 = (f32[2]{0:T(128)S(1)}, f32[2]{0:T(128)}, u32[]{:S(2)}) copy-start(f32[2]{0:T(128)} %param.30) | copy-start | bytes 28
  61.2 15.4 %copy-start.18 = (bf16[8,1,320,128]{3,2,1,0:T(8,128)(2,1)S(1)}, bf16[8,1,320,128]{3,2,1,0:T(8,128)(2,1)}, u32[]{:S(2)}) copy-start(bf16[8,1,320,128]{3,2,1,0:T(8,128)(2,1)} %param.32) | copy-start | bytes 1966084
  63.2 10.2 %all-to-all-start.1 = ((f32[8,8,512]{2,1,0:T(8,128)}), f32[8,8,512]{2,1,0:T(8,128)S(1)}, u32[]{:S(2)}, u32[]{:S(2)}) async-start(f32[8,8,512]{2,1,0:T(8,128)} %fusion.18), calls=%async_computation.1 | async-start | bytes 262144 | tf_op jit(solution)/shard_map/all_to_all | solution.py:28
  67.3 9.6 %copy-start.16 = (f32[128]{0:T(128)S(1)}, f32[128]{0:T(128)}, u32[]{:S(2)}) copy-start(f32[128]{0:T(128)} %param.34) | copy-start | bytes 1540
  76.6 9.7 %copy-start.12 = (f32[8,2]{0,1:T(2,128)S(1)}, f32[8,2]{0,1:T(2,128)}, u32[]{:S(2)}) copy-start(f32[8,2]{0,1:T(2,128)} %param.42) | copy-start | bytes 196
  76.9 14.2 %copy-start.7 = (bf16[8,2048]{1,0:T(8,128)(2,1)S(1)}, bf16[8,2048]{1,0:T(8,128)(2,1)}, u32[]{:S(2)}) copy-start(bf16[8,2048]{1,0:T(8,128)(2,1)} %param.23) | copy-start | bytes 98308
  76.9 14.8 %copy-start.9 = (f32[2048]{0:T(1024)S(1)}, f32[2048]{0:T(1024)}, u32[]{:S(2)}) copy-start(f32[2048]{0:T(1024)} %param.36) | copy-start | bytes 24580
  82.2 8.8 %all-to-all-start.2 = ((bf16[4,8,2048]{2,1,0:T(8,128)(2,1)}), bf16[4,8,2048]{2,1,0:T(8,128)(2,1)S(1)}, u32[]{:S(2)}, u32[]{:S(2)}) async-start(bf16[4,8,2048]{2,1,0:T(8,128)(2,1)} %broadcast_in_dim.27), calls=%async_computation.2 | async-start | bytes 262144 | tf_op jit(solution)/shard_map/all_to_all | solution.py:28
  91.1 0.6 copy-start.3
  91.8 44.3 %copy-start.5 = (bf16[8,2048]{1,0:T(8,128)(2,1)}, bf16[8,2048]{1,0:T(8,128)(2,1)S(1)}, u32[]{:S(2)}) copy-start(bf16[8,2048]{1,0:T(8,128)(2,1)S(1)} %multiply_convert_fusion.2) | copy-start | bytes 98308
  132.6 18.4 %all-to-all-start.4 = ((bf16[4,256,512]{1,2,0:T(8,128)(2,1)}), bf16[4,256,512]{1,2,0:T(8,128)(2,1)S(1)}, u32[]{:S(2)}, u32[]{:S(2)}) async-start(bf16[4,256,512]{1,2,0:T(8,128)(2,1)} %broadcast_in_dim.31), calls=%async_computation.4 | async-start | bytes 2097152 | tf_op jit(solution)/shard_map/all_to_all | solution.py:28
  136.2 17.0 %copy-start.1 = (bf16[1,2048,176]{1,2,0:T(8,128)(2,1)S(1)}, bf16[1,2048,176]{1,2,0:T(8,128)(2,1)}, u32[]{:S(2)}) copy-start(bf16[1,2048,176]{1,2,0:T(8,128)(2,1)} %param.44) | copy-start | bytes 2162692
  155.2 0.8 copy-start.8
  177.0 8.7 %copy-start.4 = (bf16[8,2048]{1,0:T(8,128)(2,1)S(1)}, bf16[8,2048]{1,0:T(8,128)(2,1)}, u32[]{:S(2)}) copy-start(bf16[8,2048]{1,0:T(8,128)(2,1)} %copy-done.3) | copy-start | bytes 98308
  177.0 8.8 %copy-start.6 = (bf16[8,2048]{1,0:T(8,128)(2,1)S(1)}, bf16[8,2048]{1,0:T(8,128)(2,1)}, u32[]{:S(2)}) copy-start(bf16[8,2048]{1,0:T(8,128)(2,1)} %copy-done.5) | copy-start | bytes 98308
  177.0 8.8 %copy-start.10 = (f32[2048]{0:T(1024)S(1)}, f32[2048]{0:T(1024)}, u32[]{:S(2)}) copy-start(f32[2048]{0:T(1024)} %param.40) | copy-start | bytes 24580
  178.0 30.3 %all-to-all-start.6 = ((bf16[128,2,512]{2,1,0:T(2,128)(2,1)}), bf16[128,2,512]{2,1,0:T(2,128)(2,1)S(1)}, u32[]{:S(2)}, u32[]{:S(2)}) async-start(bf16[128,2,512]{2,1,0:T(2,128)(2,1)} %reshape.345), calls=%async_computation.6 | async-start | bytes 524288 | tf_op jit(solution)/shard_map/all_to_all | solution.py:28
Sparse Core Ops, SparseCore 0:
  43.1 36.1 all-gather.2
  81.5 36.5 all-gather.4
where the time goes:
time: 217 us; the launch traced here: 216 us
  blocking collectives  86.7 us (40%)
  waiting for transfers between devices  50 us (23%)
  starting transfers between devices  31.1 us (14%)
  local copies, waits for them, and re-layouts  16.3 us (8%)
  between operations  13.9 us (6%)
  matrix products  13.4 us (6%)
  other arithmetic  4.68 us (2%)
    all_to_all x2, blocking collectives, exchange(): return lax.all_to_all(values, axes, split_axis=0, concat_axis=0, tiled=True)  55.9 us
    all_to_all x5, waiting for transfers between devices, exchange(): return lax.all_to_all(values, axes, split_axis=0, concat_axis=0, tiled=True)  47.6 us
    all_to_all x5, starting transfers between devices, exchange(): return lax.all_to_all(values, axes, split_axis=0, concat_axis=0, tiled=True)  31.1 us
    all_gather x1, blocking collectives, shards(): held = lax.all_gather(shard, Z, axis=0, tiled=True)  30.8 us
    unnamed x46, local copies, waits for them, and re-layouts  6.65 us
  transfers between devices with their start and end apart: 7, of which 6 were waited for; matrix products, arithmetic and copies ran while one was open for 10% of the time, Pallas kernels for 0%

commit v1 on v0

--- a/solution.py
+++ b/solution.py
@@ -2,6 +2,7 @@
 import jax.numpy as jnp
 from jax import lax
 from jax.sharding import Mesh, PartitionSpec as P
+from jax.lax import all_to_all, axis_size
 
 SUB = 64
 VD = 128
@@ -142,6 +143,13 @@
     expert_up,
     expert_down,
 ):
+
+    def move_spot(array_in, mesh_ax):
+        u1 = jnp.concatenate(
+            all_to_all(jnp.stack([array_in] * axis_size(mesh_ax), axis=0), mesh_ax, 0, 0), axis=0
+        )
+        return u1
+
     residual = tokens.astype(jnp.float32)
     normed = rms_scale(residual, norm_gain).astype(jnp.bfloat16)
     width = residual.shape[1]
@@ -162,7 +170,7 @@
         ),
         axis=1,
     )
-    held = lax.all_gather(shard, Z, axis=0, tiled=True)
+    held = move_spot(shard, mesh_ax=Z)
     out_held = lax.all_gather(held[:, 512:768], XC, axis=0, tiled=True)
     dense_held = lax.all_gather(held[:, 768:], XC, axis=0, tiled=True)
     partial_rows = jnp.dot(spread, held[:, :512], preferred_element_type=jnp.float32)

time: 217 us -> 233 us (1.074)
  waiting for transfers between devices: 50 us -> 84.7 us
  blocking collectives: 86.7 us -> 55.5 us
  starting transfers between devices: 31.1 us -> 44.9 us
    all_to_all x0 -> x1, waiting for transfers between devices: none -> 33.5 us  [move_spot(): all_to_all(jnp.stack([array_in] * axis_size(mesh_ax), axis=0), mesh_ax, 0...]
    all_gather x1 -> x0, blocking collectives: 30.8 us -> none  [shards(): held = lax.all_gather(shard, Z, axis=0, tiled=True)]
    all_to_all x0 -> x1, starting transfers between devices: none -> 14.8 us  [move_spot(): all_to_all(jnp.stack([array_in] * axis_size(mesh_ax), axis=0), mesh_ax, 0...]
    unnamed x46 -> x50, local copies, waits for them, and re-layouts: 6.65 us -> 6.7 us
  transfers between devices with their start and end apart: 7 -> 8, of which waited for: 6 -> 7; matrix products, arithmetic and copies ran while one was open for 10% -> 8% of each run, Pallas kernels for 0% -> 0%
where the time goes in v1:
time: 233 us; the launch traced here: 232 us
  waiting for transfers between devices  84.7 us (36%)
  blocking collectives  55.5 us (24%)
  starting transfers between devices  44.9 us (19%)
  local copies, waits for them, and re-layouts  17.4 us (7%)
  between operations  13.9 us (6%)
  matrix products  12.3 us (5%)
  other arithmetic  3.14 us (1%)
    all_to_all x2, blocking collectives, exchange(): return lax.all_to_all(values, axes, split_axis=0, concat_axis=0, tiled=True)  55.5 us
    all_to_all x5, waiting for transfers between devices, exchange(): return lax.all_to_all(values, axes, split_axis=0, concat_axis=0, tiled=True)  47.5 us
    all_to_all x1, waiting for transfers between devices, move_spot(): all_to_all(jnp.stack([array_in] * axis_size(mesh_ax), axis=0), mesh_ax, 0...  33.5 us
    all_to_all x5, starting transfers between devices, exchange(): return lax.all_to_all(values, axes, split_axis=0, concat_axis=0, tiled=True)  30.1 us
    all_to_all x1, starting transfers between devices, move_spot(): all_to_all(jnp.stack([array_in] * axis_size(mesh_ax), axis=0), mesh_ax, 0...  14.8 us
    unnamed x50, local copies, waits for them, and re-layouts  6.7 us
  transfers between devices with their start and end apart: 8, of which 7 were waited for; matrix products, arithmetic and copies ran while one was open for 8% of the time, Pallas kernels for 0%

profile of v1, /device:TPU:33, one launch (start us, length us, event | category | flops | bytes accessed | tf_op | source)
XLA Modules:
  0.0 231.8 jit_solution(7966165794464255305)
XLA Ops:
  6.5 0.8 constant_dynamic-update-slice_fusion.6
  7.3 0.7 constant_dynamic-update-slice_fusion.5
  8.0 0.7 constant_dynamic-update-slice_fusion.4
  8.7 0.7 constant_dynamic-update-slice_fusion.3
  9.4 0.7 constant_dynamic-update-slice_fusion.2
  10.1 0.7 constant_dynamic-update-slice_fusion.1
  10.8 0.7 constant_dynamic-update-slice_fusion
  11.5 1.0 stack.2
  12.5 14.8 %all-to-all-start.1 = ((bf16[16,16,1536]{2,1,0:T(8,128)(2,1)}), bf16[16,16,1536]{2,1,0:T(8,128)(2,1)S(1)}, u32[]{:S(2)}, u32[]{:S(2)}) async-start(bf16[16,16,1536]{2,1,0:T(8,128)(2,1)} %stack.2), calls=%async_computation.1 | async-start | bytes 1572864 | tf_op jit(solution)/shard_map/all_to_all | solution.py:149
  27.3 0.1 fusion.25
  27.4 33.5 %all-to-all-done.1 = bf16[16,16,1536]{2,1,0:T(8,128)(2,1)S(1)} async-done(((bf16[16,16,1536]{2,1,0:T(8,128)(2,1)}), bf16[16,16,1536]{2,1,0:T(8,128)(2,1)S(1)}, u32[]{:S(2)}, u32[]{:S(2)}) %all-to-all-start.1) | async-done | bytes 786464 | tf_op jit(solution)/shard_map/all_to_all | solution.py:149
  61.0 0.7 slice.73
  61.8 0.2 reshape.339
  62.0 0.9 reshape_reshape.3
  62.9 10.9 %all-to-all-start = ((bf16[8,8,256]{2,1,0:T(8,128)(2,1)}), bf16[8,8,256]{2,1,0:T(8,128)(2,1)S(1)}, u32[]{:S(2)}, u32[]{:S(2)}) async-start(bf16[8,8,256]{2,1,0:T(8,128)(2,1)} %bitcast.3), calls=%async_computation | async-start | bytes 65536 | tf_op jit(solution)/shard_map/all_to_all | solution.py:29
  73.8 1.2 copy.94
  75.1 0.1 fusion.6
  75.3 1.3 convert_multiply_fusion
  76.6 0.2 reduce_sum.137
  76.9 1.6 all-to-all-done
  78.5 0.9 fusion.18
  79.4 4.0 %all-to-all-start.2 = ((f32[8,8,512]{2,1,0:T(8,128)}), f32[8,8,512]{2,1,0:T(8,128)S(1)}, u32[]{:S(2)}, u32[]{:S(2)}) async-start(f32[8,8,512]{2,1,0:T(8,128)} %fusion.18), calls=%async_computation.2 | async-start | bytes 262144 | tf_op jit(solution)/shard_map/all_to_all | solution.py:29
  83.4 0.8 slice.74
  84.3 5.2 %all-to-all-done.2 = f32[8,8,512]{2,1,0:T(8,128)S(1)} async-done(((f32[8,8,512]{2,1,0:T(8,128)}), f32[8,8,512]{2,1,0:T(8,128)S(1)}, u32[]{:S(2)}, u32[]{:S(2)}) %all-to-all-start.2) | async-done | bytes 131104 | tf_op jit(solution)/shard_map/all_to_all | solution.py:29
  89.8 0.1 reduce_sum.140
  90.2 0.1 fusion.36
  90.3 0.1 copy.112
  90.5 0.4 fusion.57
  90.9 0.1 copy.97
  91.2 0.1 copy.99
  91.4 0.4 multiply_reduce_fusion.2
  91.9 3.6 %all-gather.3.cloned.1.call-done = bf16[2048,256]{1,0:T(8,128)(2,1)} async-done(((bf16[256,256]{1,0:T(8,128)(2,1)}), bf16[2048,256]{1,0:T(8,128)(2,1)}) %all-gather.3.cloned.1.call-update) | async-done | bytes 1048592 | tf_op jit(solution)/shard_map/all_gather | solution.py:174
  95.5 1.6 convolution_convert_fusion.2
  97.1 0.2 reshape.345
  97.4 0.3 broadcast_in_dim.26
  97.7 0.7 broadcast_in_dim.27
  98.4 4.0 %all-to-all-start.3 = ((bf16[4,8,2048]{2,1,0:T(8,128)(2,1)}), bf16[4,8,2048]{2,1,0:T(8,128)(2,1)S(1)}, u32[]{:S(2)}, u32[]{:S(2)}) async-start(bf16[4,8,2048]{2,1,0:T(8,128)(2,1)} %broadcast_in_dim.27), calls=%async_computation.3 | async-start | bytes 262144 | tf_op jit(solution)/shard_map/all_to_all | solution.py:29
  102.4 4.7 %all-to-all-done.3 = bf16[4,8,2048]{2,1,0:T(8,128)(2,1)S(1)} async-done(((bf16[4,8,2048]{2,1,0:T(8,128)(2,1)}), bf16[4,8,2048]{2,1,0:T(8,128)(2,1)S(1)}, u32[]{:S(2)}, u32[]{:S(2)}) %all-to-all-start.3) | async-done | bytes 131104 | tf_op jit(solution)/shard_map/all_to_all | solution.py:29
  107.2 0.1 multiply_reduce_fusion.1
  107.4 0.5 copy-done.4
  108.0 0.2 convolution_convert_fusion.3
  108.2 0.1 broadcast_in_dim.29
  108.3 38.7 %all_to_all.40 = bf16[128,2,512]{2,1,0:T(2,128)(2,1)S(1)} all-to-all(bf16[128,2,512]{2,1,0:T(2,128)(2,1)S(1)} %bitcast.141), channel_id=1, replica_groups=mesh['b'=8,'zp'=2,'x'=4,'c'=2,'tp'=4] {'b','zp','x','c'}, dimensions={0} | all-to-all | bytes 524288 | tf_op jit(solution)/shard_map/all_to_all | solution.py:29
  147.0 0.1 broadcast_in_dim.30
  147.1 0.1 copy.106
  147.3 1.1 broadcast_in_dim.31
  148.3 3.5 %all-to-all-start.5 = ((bf16[4,256,512]{1,2,0:T(8,128)(2,1)}), bf16[4,256,512]{1,2,0:T(8,128)(2,1)S(1)}, u32[]{:S(2)}, u32[]{:S(2)}) async-start(bf16[4,256,512]{1,2,0:T(8,128)(2,1)} %broadcast_in_dim.31), calls=%async_computation.5 | async-start | bytes 2097152 | tf_op jit(solution)/shard_map/all_to_all | solution.py:29
  151.9 0.2 reshape.348
  152.1 0.9 reshape.349
  153.1 13.6 %all-to-all-done.5 = bf16[4,256,512]{1,2,0:T(8,128)(2,1)S(1)} async-done(((bf16[4,256,512]{1,2,0:T(8,128)(2,1)}), bf16[4,256,512]{1,2,0:T(8,128)(2,1)S(1)}, u32[]{:S(2)}, u32[]{:S(2)}) %all-to-all-start.5) | async-done | bytes 1048608 | tf_op jit(solution)/shard_map/all_to_all | solution.py:29
  166.7 2.1 fusion.15
  168.8 2.1 convolution_convert_fusion
  171.1 0.6 copy-done.9
  171.7 2.0 fusion
  173.7 1.6 convolution_convert_fusion.1
  175.3 0.2 reshape.350
  175.6 0.3 concatenate.13
  176.0 16.8 %all_to_all.41 = bf16[4,264,512]{2,1,0:T(8,128)(2,1)S(1)} all-to-all(bf16[4,264,512]{2,1,0:T(8,128)(2,1)S(1)} %maximum_bitcast_fusion), channel_id=1, replica_groups=mesh['b'=8,'zp'=2,'x'=4,'c'=2,'tp'=4] {'tp'}, dimensions={0} | all-to-all | bytes 2162688 | tf_op jit(solution)/shard_map/all_to_all | solution.py:29
  192.8 0.2 convert_reduce_fusion
  193.0 0.8 reshape.351
  193.7 7.7 %all-to-all-start.7 = ((bf16[128,2,512]{2,1,0:T(2,128)(2,1)}), bf16[128,2,512]{2,1,0:T(2,128)(2,1)S(1)}, u32[]{:S(2)}, u32[]{:S(2)}) async-start(bf16[128,2,512]{2,1,0:T(2,128)(2,1)} %reshape.351), calls=%async_computation.7 | async-start | bytes 524288 | tf_op jit(solution)/shard_map/all_to_all | solution.py:29
  201.5 0.1 multiply_reduce_fusion
  201.7 22.4 %all-to-all-done.7 = bf16[128,2,512]{2,1,0:T(2,128)(2,1)S(1)} async-done(((bf16[128,2,512]{2,1,0:T(2,128)(2,1)}), bf16[128,2,512]{2,1,0:T(2,128)(2,1)S(1)}, u32[]{:S(2)}, u32[]{:S(2)}) %all-to-all-start.7) | async-done | bytes 262176 | tf_op jit(solution)/shard_map/all_to_all | solution.py:29
  224.2 0.8 fusion.5
  (96 shorter events, 2.5 us)
Async XLA Ops:
  6.5 162.3 %copy-start = (bf16[1,176,2048]{2,1,0:T(8,128)(2,1)S(1)}, bf16[1,176,2048]{2,1,0:T(8,128)(2,1)}, u32[]{:S(2)}) copy-start(bf16[1,176,2048]{2,1,0:T(8,128)(2,1)} %param.45) | copy-start | bytes 2162692
  6.5 20.8 %copy-start.8 = (bf16[8,2048]{1,0:T(8,128)(2,1)S(1)}, bf16[8,2048]{1,0:T(8,128)(2,1)}, u32[]{:S(2)}) copy-start(bf16[8,2048]{1,0:T(8,128)(2,1)} %param.23) | copy-start | bytes 98308
  6.5 55.2 %copy-start.10 = (f32[2048]{0:T(1024)S(1)}, f32[2048]{0:T(1024)}, u32[]{:S(2)}) copy-start(f32[2048]{0:T(1024)} %param.24) | copy-start | bytes 24580
  12.4 61.3 %copy-start.3 = (bf16[8,1,320,128]{3,2,1,0:T(8,128)(2,1)S(1)}, bf16[8,1,320,128]{3,2,1,0:T(8,128)(2,1)}, u32[]{:S(2)}) copy-start(bf16[8,1,320,128]{3,2,1,0:T(8,128)(2,1)} %param.31) | copy-start | bytes 1966084
  12.5 48.5 %all-to-all-start.1 = ((bf16[16,16,1536]{2,1,0:T(8,128)(2,1)}), bf16[16,16,1536]{2,1,0:T(8,128)(2,1)S(1)}, u32[]{:S(2)}, u32[]{:S(2)}) async-start(bf16[16,16,1536]{2,1,0:T(8,128)(2,1)} %stack.2), calls=%async_computation.1 | async-start | bytes 1572864 | tf_op jit(solution)/shard_map/all_to_all | solution.py:149
  27.2 47.7 %copy-start.13 = (s32[8,2]{0,1:T(2,128)S(1)}, s32[8,2]{0,1:T(2,128)}, u32[]{:S(2)}) copy-start(s32[8,2]{0,1:T(2,128)} %param.41) | copy-start | bytes 196
  27.2 68.3 %all-gather.3.cloned.1.call-start = ((), (), s32[]{:S(2)}) async-start(), calls=%async_computation.8 | async-start | bytes 1179648 | tf_op jit(solution)/shard_map/all_gather | solution.py:174
  62.9 15.6 %all-to-all-start = ((bf16[8,8,256]{2,1,0:T(8,128)(2,1)}), bf16[8,8,256]{2,1,0:T(8,128)(2,1)S(1)}, u32[]{:S(2)}, u32[]{:S(2)}) async-start(bf16[8,8,256]{2,1,0:T(8,128)(2,1)} %bitcast.3), calls=%async_computation | async-start | bytes 65536 | tf_op jit(solution)/shard_map/all_to_all | solution.py:29
  76.6 6.8 %copy-start.16 = (s32[8]{0:T(128)S(1)}, s32[8]{0:T(128)}, u32[]{:S(2)}) copy-start(s32[8]{0:T(128)} %param.33) | copy-start | bytes 100
  76.6 13.4 %copy-start.17 = (f32[64]{0:T(128)S(1)}, f32[64]{0:T(128)}, u32[]{:S(2)}) copy-start(f32[64]{0:T(128)} %param.29) | copy-start | bytes 772
  76.6 13.5 %copy-start.15 = (f32[64]{0:T(128)S(1)}, f32[64]{0:T(128)}, u32[]{:S(2)}) copy-start(f32[64]{0:T(128)} %param.28) | copy-start | bytes 772
  76.8 13.6 %copy-start.1 = (bf16[8,1,320,128]{2,3,0,1:T(8,128)(2,1)S(1)}, bf16[8,1,320,128]{2,3,0,1:T(8,128)(2,1)}, u32[]{:S(2)}) copy-start(bf16[8,1,320,128]{2,3,0,1:T(8,128)(2,1)} %copy.94) | copy-start | bytes 1966084
  79.4 10.1 %all-to-all-start.2 = ((f32[8,8,512]{2,1,0:T(8,128)}), f32[8,8,512]{2,1,0:T(8,128)S(1)}, u32[]{:S(2)}, u32[]{:S(2)}) async-start(f32[8,8,512]{2,1,0:T(8,128)} %fusion.18), calls=%async_computation.2 | async-start | bytes 262144 | tf_op jit(solution)/shard_map/all_to_all | solution.py:29
  83.4 87.7 %all-gather.5.cloned.1.call-start = ((), (), s32[]{:S(2)}) async-start(), calls=%async_computation.9 | async-start | bytes 3538944 | tf_op jit(solution)/shard_map/all_gather | solution.py:175
  83.4 7.6 %copy-start.19 = (f32[2]{0:T(128)S(1)}, f32[2]{0:T(128)}, u32[]{:S(2)}) copy-start(f32[2]{0:T(128)} %param.30) | copy-start | bytes 28
  84.2 7.2 %copy-start.20 = (bf16[8,1,320,128]{3,2,1,0:T(8,128)(2,1)S(1)}, bf16[8,1,320,128]{3,2,1,0:T(8,128)(2,1)}, u32[]{:S(2)}) copy-start(bf16[8,1,320,128]{3,2,1,0:T(8,128)(2,1)} %param.32) | copy-start | bytes 1966084
  84.2 7.5 %copy-start.18 = (f32[128]{0:T(128)S(1)}, f32[128]{0:T(128)}, u32[]{:S(2)}) copy-start(f32[128]{0:T(128)} %param.34) | copy-start | bytes 1540
  91.4 11.0 %copy-start.14 = (f32[8,2]{0,1:T(2,128)S(1)}, f32[8,2]{0,1:T(2,128)}, u32[]{:S(2)}) copy-start(f32[8,2]{0,1:T(2,128)} %param.42) | copy-start | bytes 196
  91.8 16.1 %copy-start.11 = (f32[2048]{0:T(1024)S(1)}, f32[2048]{0:T(1024)}, u32[]{:S(2)}) copy-start(f32[2048]{0:T(1024)} %param.36) | copy-start | bytes 24580
  98.4 8.8 %all-to-all-start.3 = ((bf16[4,8,2048]{2,1,0:T(8,128)(2,1)}), bf16[4,8,2048]{2,1,0:T(8,128)(2,1)S(1)}, u32[]{:S(2)}, u32[]{:S(2)}) async-start(bf16[4,8,2048]{2,1,0:T(8,128)(2,1)} %broadcast_in_dim.27), calls=%async_computation.3 | async-start | bytes 262144 | tf_op jit(solution)/shard_map/all_to_all | solution.py:29
  107.2 0.6 copy-start.4
  107.9 43.9 %copy-start.6 = (bf16[8,2048]{1,0:T(8,128)(2,1)}, bf16[8,2048]{1,0:T(8,128)(2,1)S(1)}, u32[]{:S(2)}) copy-start(bf16[8,2048]{1,0:T(8,128)(2,1)S(1)} %multiply_convert_fusion.2) | copy-start | bytes 98308
  148.3 18.4 %all-to-all-start.5 = ((bf16[4,256,512]{1,2,0:T(8,128)(2,1)}), bf16[4,256,512]{1,2,0:T(8,128)(2,1)S(1)}, u32[]{:S(2)}, u32[]{:S(2)}) async-start(bf16[4,256,512]{1,2,0:T(8,128)(2,1)} %broadcast_in_dim.31), calls=%async_computation.5 | async-start | bytes 2097152 | tf_op jit(solution)/shard_map/all_to_all | solution.py:29
  151.9 17.0 %copy-start.2 = (bf16[1,2048,176]{1,2,0:T(8,128)(2,1)S(1)}, bf16[1,2048,176]{1,2,0:T(8,128)(2,1)}, u32[]{:S(2)}) copy-start(bf16[1,2048,176]{1,2,0:T(8,128)(2,1)} %param.44) | copy-start | bytes 2162692
  170.9 0.8 copy-start.9
  192.7 8.7 %copy-start.5 = (bf16[8,2048]{1,0:T(8,128)(2,1)S(1)}, bf16[8,2048]{1,0:T(8,128)(2,1)}, u32[]{:S(2)}) copy-start(bf16[8,2048]{1,0:T(8,128)(2,1)} %copy-done.4) | copy-start | bytes 98308
  192.7 8.8 %copy-start.7 = (bf16[8,2048]{1,0:T(8,128)(2,1)S(1)}, bf16[8,2048]{1,0:T(8,128)(2,1)}, u32[]{:S(2)}) copy-start(bf16[8,2048]{1,0:T(8,128)(2,1)} %copy-done.6) | copy-start | bytes 98308
  192.7 8.8 %copy-start.12 = (f32[2048]{0:T(1024)S(1)}, f32[2048]{0:T(1024)}, u32[]{:S(2)}) copy-start(f32[2048]{0:T(1024)} %param.40) | copy-start | bytes 24580
  193.7 30.3 %all-to-all-start.7 = ((bf16[128,2,512]{2,1,0:T(2,128)(2,1)}), bf16[128,2,512]{2,1,0:T(2,128)(2,1)S(1)}, u32[]{:S(2)}, u32[]{:S(2)}) async-start(bf16[128,2,512]{2,1,0:T(2,128)(2,1)} %reshape.351), calls=%async_computation.7 | async-start | bytes 524288 | tf_op jit(solution)/shard_map/all_to_all | solution.py:29
Sparse Core Ops, SparseCore 0:
  61.8 33.6 all-gather.2
  97.6 36.0 all-gather.4
